TPU v7x, 512 devices: a whole 4x8x8 slice. The times are simulated.
512 devices in a mesh: rep: 2 (over z_hi), fs: 32 (over z_lo, y), tp: 8 (over x, core).
Axes of the slice: x: 4, y: 8, z: 8 (z_hi: 2, z_lo: 4; z = z_hi * 4 + z_lo), core: 2. Of those that a mesh axis runs over, the one named last changes fastest.
Arguments:
- pre_gate: bfloat16 [49152, 4096], P(('rep', 'fs'), 'tp'), may hold values from -6 to 6
- pre_linear: bfloat16 [49152, 4096], P(('rep', 'fs'), 'tp'), may hold values from -6 to 6
- taps_gate: float32 [3, 4096], P(None, 'tp'), may hold values from -3.5 to 3.5
- taps_linear: float32 [3, 4096], P(None, 'tp'), may hold values from -3.5 to 3.5
- bias_gate: float32 [4096], P('tp'), may hold values from -3 to 3
- bias_linear: float32 [4096], P('tp'), may hold values from -3 to 3
- down_weight: bfloat16 [4096, 2048], P('tp', 'fs'), may hold values from -0.09375 to 0.09375
- out_grad: bfloat16 [49152, 2048], P(('rep', 'fs')), may hold values from -8 to 8
Outputs:
- grad_gate: bfloat16 [49152, 4096], P(('rep', 'fs'), 'tp')
- grad_linear: bfloat16 [49152, 4096], P(('rep', 'fs'), 'tp')
- grad_taps_gate: float32 [3, 4096], P(None, 'tp')
- grad_taps_linear: float32 [3, 4096], P(None, 'tp')
- grad_bias_gate: float32 [4096], P('tp')
- grad_bias_linear: float32 [4096], P('tp')
- grad_down: float32 [4096, 2048], P('tp', 'fs')
- row_norms: float32 [4096], P('tp')
All inputs are finite; a program needn't handle non-finite values.
Results may differ from a plain program's by a relative error of at most 0.0031.
Values may be sent and summed in bfloat16 or wider, within the bound.
A program may use at most 64 MiB of HBM per device.

v0:
```python
import jax
import jax.numpy as jnp
from jax import lax
from jax.sharding import Mesh
from jax.sharding import PartitionSpec as P

FS = ("fs_0", "fs_1")
REP_FS = ("rep", "fs_0", "fs_1")


def joined_along(parts, dim):
    lengths = list(parts.shape[1:])
    lengths[dim] *= parts.shape[0]
    return jnp.moveaxis(parts, 0, dim).reshape(lengths)


def copy_for_each(shard, axis):
    count = lax.axis_size(axis)
    return lax.all_to_all(
        jnp.broadcast_to(shard[None], (count, *shard.shape)), axis, 0, 0, tiled=True
    )


def gather_directly(shard, axis, dim):
    return joined_along(copy_for_each(shard, axis), dim)


def by_axis(shard, axes):
    for axis in axes:
        shard = lax.psum(shard, axis)
    return shard


def sum_in_order(parts, axes, sequence):
    inside = parts.shape[1:]
    parts = parts.reshape(*(lax.axis_size(a) for a in axes), *inside)
    parts = jnp.moveaxis(parts, sequence, range(len(axes))).reshape(-1, *inside)
    for k in sequence:
        parts = lax.psum_scatter(parts, axes[k], scatter_dimension=0, tiled=True)
    return parts[0]


def split_up(shard, dim, count):
    lengths = shard.shape
    parts = shard.reshape(*lengths[:dim], count, lengths[dim] // count, *lengths[dim + 1 :])
    return jnp.moveaxis(parts, dim, 0)


def scatter_axes(shard, axes, sequence, dim):
    count = lax.axis_size(axes)
    return sum_in_order(split_up(shard, dim, count), axes, sequence)


def of_everyone(shard, axis):
    everything = copy_for_each(shard, axis)
    return jnp.sum(everything, axis=0)


def convolve(values, taps, bias):
    length = values.shape[0]
    padded = jnp.pad(values, ((2, 0), (0, 0)))
    return (
        taps[0] * padded[0:length]
        + taps[1] * padded[1 : length + 1]
        + taps[2] * padded[2 : length + 2]
        + bias
    )


def convolve_back(grads, taps):
    length = grads.shape[0]
    padded = jnp.pad(grads, ((0, 2), (0, 0)))
    return (
        taps[0] * padded[2 : length + 2]
        + taps[1] * padded[1 : length + 1]
        + taps[2] * padded[0:length]
    )


def tap_grads(grads, values):
    length = values.shape[0]
    padded = jnp.pad(values, ((2, 0), (0, 0)))
    return jnp.stack([jnp.sum(grads * padded[j : j + length], axis=0) for j in range(3)])


def local(
    pre_gate, pre_linear, taps_gate, taps_linear, bias_gate, bias_linear, down_weight, out_grad
):
    gate_in = pre_gate.astype(jnp.float32)
    linear_in = pre_linear.astype(jnp.float32)
    gate_pre = convolve(gate_in, taps_gate, bias_gate)
    linear_pre = convolve(linear_in, taps_linear, bias_linear)
    sigma = jax.nn.sigmoid(gate_pre)
    silu_val = gate_pre * sigma
    hidden = (silu_val * linear_pre).astype(jnp.bfloat16)
    gathered = gather_directly(down_weight, FS, 1)
    grad_hidden = lax.dot_general(
        out_grad, gathered, (((1,), (1,)), ((), ())), preferred_element_type=jnp.float32
    )
    grad_gate_pre = grad_hidden * linear_pre * sigma * (1.0 + gate_pre * (1.0 - sigma))
    grad_linear_pre = grad_hidden * silu_val
    grad_gate = convolve_back(grad_gate_pre, taps_gate).astype(jnp.bfloat16)
    grad_linear = convolve_back(grad_linear_pre, taps_linear).astype(jnp.bfloat16)
    conv_parts = (
        tap_grads(grad_gate_pre, gate_in),
        tap_grads(grad_linear_pre, linear_in),
        jnp.sum(grad_gate_pre, axis=0),
        jnp.sum(grad_linear_pre, axis=0),
    )
    grad_taps_gate, grad_taps_linear, grad_bias_gate, grad_bias_linear = (
        by_axis(conv_parts[0], REP_FS),
        by_axis(conv_parts[1], REP_FS),
        by_axis(conv_parts[2], REP_FS),
        by_axis(conv_parts[3], REP_FS),
    )
    partial_grad = scatter_axes(
        lax.dot_general(
            out_grad, hidden, (((0,), (0,)), ((), ())), preferred_element_type=jnp.float32
        ),
        FS,
        (1, 0),
        0,
    )
    summed = of_everyone(partial_grad, "rep")
    grad_down = summed.T
    row_norms = by_axis(jnp.sum(grad_down * grad_down, axis=1), FS)
    return (
        grad_gate,
        grad_linear,
        grad_taps_gate,
        grad_taps_linear,
        grad_bias_gate,
        grad_bias_linear,
        grad_down,
        row_norms,
    )


def solution(mesh):
    split = Mesh(
        mesh.devices.reshape(mesh.shape["rep"], 4, 8, mesh.shape["tp"]),
        ("rep", "fs_0", "fs_1", "tp"),
    )
    in_specs = (
        P(REP_FS, "tp"),
        P(REP_FS, "tp"),
        P(None, "tp"),
        P(None, "tp"),
        P("tp"),
        P("tp"),
        P("tp", FS),
        P(REP_FS, None),
    )
    out_specs = (
        P(REP_FS, "tp"),
        P(REP_FS, "tp"),
        P(None, "tp"),
        P(None, "tp"),
        P("tp"),
        P("tp"),
        P("tp", FS),
        P("tp"),
    )
    return jax.shard_map(local, mesh=split, in_specs=in_specs, out_specs=out_specs, check_vma=False)
```

profile of v0, /device:TPU:2, one launch (start us, length us, event | category | flops | bytes accessed | tf_op | source)
XLA Modules:
  0.0 261.0 jit_solution(16937942078931800513)
XLA Ops:
  7.2 0.0 copy-start
  7.2 2.5 broadcast_in_dim.6
  9.7 13.0 %all-to-all-start = ((bf16[32,512,64]{1,2,0:T(8,128)(2,1)}), bf16[32,512,64]{1,2,0:T(8,128)(2,1)}, u32[]{:S(2)}, u32[]{:S(2)}) async-start(bf16[32,512,64]{1,2,0:T(8,128)(2,1)} %broadcast_in_dim.6), calls=%async_computation | async-start | bytes 4194304 | tf_op jit(solution)/shard_map/all_to_all | solution.py:19
  22.8 0.0 reduce-scatter.3.cloned.1.call-start
  22.8 0.0 copy-start.4
  22.8 2.6 convert_element_type.24
  25.4 0.0 copy-done.4
  25.4 0.0 copy-start.6
  25.4 0.0 copy-start.7
  25.4 0.0 copy-start.9
  25.4 1.4 convert_element_type.23
  26.8 0.0 copy-done.6
  26.9 0.0 copy-done.7
  26.9 46.6 %all-to-all-done = bf16[32,512,64]{1,2,0:T(8,128)(2,1)} async-done(((bf16[32,512,64]{1,2,0:T(8,128)(2,1)}), bf16[32,512,64]{1,2,0:T(8,128)(2,1)}, u32[]{:S(2)}, u32[]{:S(2)}) %all-to-all-start) | async-done | bytes 2097184 | tf_op jit(solution)/shard_map/all_to_all | solution.py:19
  73.5 0.0 copy-done
  73.5 0.0 copy-done.9
  73.5 0.0 copy-start.1
  73.5 0.0 copy-start.2
  73.5 0.0 copy-start.3
  73.5 0.0 copy-start.8
  73.5 7.1 %fusion.4 = (f32[512]{0:T(512)S(1)}, f32[512]{0:T(512)S(1)}, f32[512]{0:T(512)S(1)}, f32[512]{0:T(512)S(1)}, f32[768,512]{1,0:T(8,128)S(1)}, /*index=5*/f32[768,512]{1,0:T(8,128)S(1)}, f32[768,512]{1,0:T(8,128)S(1)}) fusion(bf16[768,512]{1,0:T(8,128)(2,1)} %param.9, f32[768,512]{1,0:T(8,128)} %convert_element_type.23, f32[512]{0:T(512)S(1)} %copy-done.9, ...), kind=kOutput, calls=%fused_computation.24 | convolution fusion | flops 1618081792 | bytes 13910016 | tf_op jit(solution)/shard_map/dot_general | solution.py:97
  80.6 0.0 copy-done.1
  80.6 0.0 copy-done.2
  80.7 0.0 copy-done.3
  80.7 0.0 copy-done.8
  80.7 3.2 %fusion.5 = (f32[512]{0:T(512)S(1)}, f32[512]{0:T(512)S(1)}, f32[512]{0:T(512)S(1)}, f32[512]{0:T(512)S(1)}, f32[768,512]{1,0:T(8,128)}, /*index=5*/f32[768,512]{1,0:T(8,128)S(1)}, bf16[768,512]{1,0:T(8,128)(2,1)}) fusion(bf16[768,512]{1,0:T(8,128)(2,1)S(1)} %copy-done.3, f32[768,512]{1,0:T(8,128)S(1)} %copy-done.1, f32[768,512]{1,0:T(8,128)S(1)} %get-tuple-element.35, ...), kind=kLoop, calls=%fused_computation.25 | loop fusion | flops 11401216 | bytes 12599296 | tf_op jit(solution)/shard_map/reduce_sum | solution.py:107
  83.9 3.9 %convolution_bitcast_fusion = f32[2048,512]{0,1:T(8,128)} fusion(bf16[768,2048]{1,0:T(8,128)(2,1)S(1)} %copy-done, f32[768,512]{1,0:T(8,128)S(1)} %get-tuple-element.37, f32[768,512]{1,0:T(8,128)S(1)} %get-tuple-element.35), kind=kOutput, calls=%fused_computation | convolution fusion | flops 1612972032 | bytes 10485760 | tf_op jit(solution)/shard_map/dot_general | solution.py:117
  87.9 5.3 %copy.19 = f32[2048,512]{1,0:T(8,128)} copy(f32[2048,512]{0,1:T(8,128)} %convolution_bitcast_fusion) | data formatting | bytes 8388608 | tf_op jit(solution)/shard_map/dot_general | solution.py:117
  93.2 4.9 %copy.20 = f32[8,4,64,512]{3,2,1,0:T(8,128)} copy(f32[8,4,64,512]{3,2,0,1:T(8,128)} %bitcast.28) | data formatting | bytes 8388608 | tf_op jit(solution)/shard_map/transpose | solution.py:37
  98.1 0.0 reduce-scatter.3.cloned.1.call-update
  98.1 0.0 reduce-scatter.5.cloned.1.call-start
  98.2 58.8 %reduce-scatter.3.cloned.1.call-done = f32[4,64,512]{2,1,0:T(8,128)} async-done(((f32[32,64,512]{2,1,0:T(8,128)}), f32[4,64,512]{2,1,0:T(8,128)}) %reduce-scatter.3.cloned.1.call-update) | async-done | bytes 524304 | tf_op jit(solution)/shard_map/reduce_scatter | solution.py:39
  157.0 0.0 reduce-scatter.5.cloned.1.call-update
  157.0 17.5 %all-reduce.6 = (f32[3,512]{1,0:T(4,128)S(1)}, f32[3,512]{1,0:T(4,128)S(1)}, f32[512]{0:T(512)}, f32[512]{0:T(512)}) all-reduce(f32[3,512]{1,0:T(4,128)S(1)} %get-tuple-element.46, f32[3,512]{1,0:T(4,128)S(1)} %get-tuple-element.47, f32[512]{0:T(512)S(1)} %get-tuple-element.16, ...), channel_id=1, replica_groups=mesh['rep'=2,'fs_0'=4,'fs_1'=8,'tp'=8] {'rep'}, use_global_device_ids=true, to_apply=%region_3.4 | all-reduce | flops 4096 | bytes 32768 | tf_op jit(solution)/shard_map/psum | solution.py:30
  174.5 14.6 %reduce-scatter.5.cloned.1.call-done = f32[1,64,512]{2,1,0:T(8,128)} async-done(((f32[4,64,512]{2,1,0:T(8,128)}), f32[1,64,512]{2,1,0:T(8,128)}) %reduce-scatter.5.cloned.1.call-update) | async-done | bytes 131088 | tf_op jit(solution)/shard_map/reduce_scatter | solution.py:39
  189.0 1.6 broadcast_in_dim.8
  190.7 4.1 %all-to-all-start.1 = ((f32[2,64,512]{2,1,0:T(8,128)}), f32[2,64,512]{2,1,0:T(8,128)S(1)}, u32[]{:S(2)}, u32[]{:S(2)}) async-start(f32[2,64,512]{2,1,0:T(8,128)} %broadcast_in_dim.8), calls=%async_computation.3 | async-start | bytes 524288 | tf_op jit(solution)/shard_map/all_to_all | solution.py:19
  194.8 4.1 %add_convert_fusion.1 = bf16[768,512]{1,0:T(8,128)(2,1)} fusion(f32[768,512]{1,0:T(8,128)} %get-tuple-element.36, f32[512]{0:T(512)S(1)} %bitcast.40, f32[512]{0:T(512)S(1)} %bitcast.42, f32[512]{0:T(512)S(1)} %bitcast.38), kind=kLoop, calls=%fused_computation.9 | loop fusion | flops 2359296 | bytes 2365440 | tf_op jit(solution)/shard_map/convert_element_type | solution.py:102
  198.9 5.5 %all-to-all-done.1 = f32[2,64,512]{2,1,0:T(8,128)S(1)} async-done(((f32[2,64,512]{2,1,0:T(8,128)}), f32[2,64,512]{2,1,0:T(8,128)S(1)}, u32[]{:S(2)}, u32[]{:S(2)}) %all-to-all-start.1) | async-done | bytes 262176 | tf_op jit(solution)/shard_map/all_to_all | solution.py:19
  204.5 0.0 copy-start.5
  204.5 19.2 %all-reduce.5 = (f32[3,512]{1,0:T(4,128)S(1)}, f32[3,512]{1,0:T(4,128)S(1)}, f32[512]{0:T(512)S(1)}, f32[512]{0:T(512)S(1)}, f32[512]{0:T(512)S(1)}) all-reduce(f32[3,512]{1,0:T(4,128)S(1)} %get-tuple-element.30, f32[3,512]{1,0:T(4,128)S(1)} %get-tuple-element.31, ...), channel_id=1, replica_groups=mesh['rep'=2,'fs_0'=4,'fs_1'=8,'tp'=8] {'fs_0'}, use_global_device_ids=true, to_apply=%region_4.5 | all-reduce | flops 4608 | bytes 36864 | tf_op jit(solution)/shard_map/psum | solution.py:30
  223.7 30.4 %all-reduce.4 = (f32[3,512]{1,0:T(4,128)}, f32[3,512]{1,0:T(4,128)}, f32[512]{0:T(512)}, f32[512]{0:T(512)}, f32[512]{0:T(512)}) all-reduce(f32[3,512]{1,0:T(4,128)S(1)} %get-tuple-element.25, f32[3,512]{1,0:T(4,128)S(1)} %get-tuple-element.26, ...), channel_id=1, replica_groups=mesh['rep'=2,'fs_0'=4,'fs_1'=8,'tp'=8] {'fs_1'}, use_global_device_ids=true, to_apply=%region_5.6 | all-reduce | flops 4608 | bytes 36864 | tf_op jit(solution)/shard_map/psum | solution.py:30
  254.1 0.0 copy-done.5
  (5 shorter events, 0.1 us)
Async XLA Ops:
  7.2 66.3 %copy-start = (bf16[768,2048]{1,0:T(8,128)(2,1)S(1)}, bf16[768,2048]{1,0:T(8,128)(2,1)}, u32[]{:S(2)}) copy-start(bf16[768,2048]{1,0:T(8,128)(2,1)} %param.15) | copy-start | bytes 9437188
  9.7 63.8 %all-to-all-start = ((bf16[32,512,64]{1,2,0:T(8,128)(2,1)}), bf16[32,512,64]{1,2,0:T(8,128)(2,1)}, u32[]{:S(2)}, u32[]{:S(2)}) async-start(bf16[32,512,64]{1,2,0:T(8,128)(2,1)} %broadcast_in_dim.6), calls=%async_computation | async-start | bytes 4194304 | tf_op jit(solution)/shard_map/all_to_all | solution.py:19
  22.8 134.2 %reduce-scatter.3.cloned.1.call-start = ((), (), s32[]{:S(2)}) async-start(), calls=%async_computation.4 | async-start | bytes 4718592 | tf_op jit(solution)/shard_map/reduce_scatter | solution.py:39
  22.8 2.6 %copy-start.4 = (bf16[768,512]{1,0:T(8,128)(2,1)S(1)}, bf16[768,512]{1,0:T(8,128)(2,1)}, u32[]{:S(2)}) copy-start(bf16[768,512]{1,0:T(8,128)(2,1)} %param.9) | copy-start | bytes 2359300
  25.4 1.4 copy-start.6
  25.4 1.4 copy-start.7
  25.4 48.1 %copy-start.9 = (f32[512]{0:T(512)S(1)}, f32[512]{0:T(512)}, u32[]{:S(2)}) copy-start(f32[512]{0:T(512)} %param.12) | copy-start | bytes 6148
  73.5 7.1 %copy-start.1 = (f32[768,512]{1,0:T(8,128)S(1)}, f32[768,512]{1,0:T(8,128)}, u32[]{:S(2)}) copy-start(f32[768,512]{1,0:T(8,128)} %convert_element_type.24) | copy-start | bytes 4718596
  73.5 7.1 %copy-start.2 = (f32[768,512]{1,0:T(8,128)S(1)}, f32[768,512]{1,0:T(8,128)}, u32[]{:S(2)}) copy-start(f32[768,512]{1,0:T(8,128)} %convert_element_type.23) | copy-start | bytes 4718596
  73.5 7.2 %copy-start.3 = (bf16[768,512]{1,0:T(8,128)(2,1)S(1)}, bf16[768,512]{1,0:T(8,128)(2,1)}, u32[]{:S(2)}) copy-start(bf16[768,512]{1,0:T(8,128)(2,1)} %param.8) | copy-start | bytes 2359300
  73.5 7.1 %copy-start.8 = (f32[512]{0:T(512)S(1)}, f32[512]{0:T(512)}, u32[]{:S(2)}) copy-start(f32[512]{0:T(512)} %param.13) | copy-start | bytes 6148
  98.1 90.9 %reduce-scatter.5.cloned.1.call-start = ((), (), s32[]{:S(2)}) async-start(), calls=%async_computation.5 | async-start | bytes 655360 | tf_op jit(solution)/shard_map/reduce_scatter | solution.py:39
  190.7 13.8 %all-to-all-start.1 = ((f32[2,64,512]{2,1,0:T(8,128)}), f32[2,64,512]{2,1,0:T(8,128)S(1)}, u32[]{:S(2)}, u32[]{:S(2)}) async-start(f32[2,64,512]{2,1,0:T(8,128)} %broadcast_in_dim.8), calls=%async_computation.3 | async-start | bytes 524288 | tf_op jit(solution)/shard_map/all_to_all | solution.py:19
  204.5 49.7 %copy-start.5 = (f32[64,512]{1,0:T(8,128)}, f32[64,512]{1,0:T(8,128)S(1)}, u32[]{:S(2)}) copy-start(f32[64,512]{1,0:T(8,128)S(1)} %reduce_sum.98) | copy-start | bytes 393220
Sparse Core Ops, SparseCore 0:
  98.2 58.7 reduce-scatter.2
  159.8 29.1 reduce-scatter.4
where the time goes:
time: 261 us
  waiting for transfers between devices  126 us (48%)
  blocking collectives  67.1 us (26%)
  starting transfers between devices  17.3 us (7%)
  local copies, waits for them, and re-layouts  14.4 us (6%)
  between operations  14.2 us (5%)
  other arithmetic  11.4 us (4%)
  matrix products  11 us (4%)
    reduce_scatter x2, waiting for transfers between devices, sum_in_order(): parts = lax.psum_scatter(parts, axes[k], scatter_dimension=0, tiled=True)  73.4 us
    psum x3, blocking collectives, by_axis(): shard = lax.psum(shard, axis)  67.1 us
    all_to_all x2, waiting for transfers between devices, copy_for_each(): lax.all_to_all(jnp.broadcast_to(shard[None], (count, *shard.shape)), axis...  52.1 us
    all_to_all x2, starting transfers between devices, copy_for_each(): lax.all_to_all(jnp.broadcast_to(shard[None], (count, *shard.shape)), axis...  17.2 us
    dot_general x1, matrix products, local(): lax.dot_general(out_grad, gathered, (((1,), (1,)), ((), ())), preferred_e...  7.1 us
    dot_general x1, local copies, waits for them, and re-layouts, local(): lax.dot_general(out_grad, hidden, (((0,), (0,)), ((), ())), preferred_ele...  5.35 us
  transfers between devices with their start and end apart: 4, of which 4 were waited for; matrix products, arithmetic and copies ran while one was open for 3% of the time, Pallas kernels for 0%

commit v1 on v0

--- a/solution.py
+++ b/solution.py
@@ -27,7 +27,7 @@
 
 def by_axis(shard, axes):
     for axis in axes:
-        shard = lax.psum(shard, axis)
+        shard = jnp.sum(lax.all_gather(shard, axis), axis=0)
     return shard
 
 

time: 261 us -> 395 us (1.51)
  blocking collectives: 67.1 us -> 209 us
  waiting for transfers between devices: 126 us -> 110 us
    all_gather x0 -> x14, blocking collectives: none -> 209 us  [by_axis(): shard = jnp.sum(lax.all_gather(shard, axis), axis=0)]
    psum x3 -> x0, blocking collectives: 67.1 us -> none  [by_axis(): shard = lax.psum(shard, axis)]
    reduce_scatter x2, waiting for transfers between devices: 73.4 us -> 58.8 us  [sum_in_order(): parts = lax.psum_scatter(parts, axes[k], scatter_dimension=0, tiled=True)]
  transfers between devices with their start and end apart: 4 -> 4, of which waited for: 4 -> 3; matrix products, arithmetic and copies ran while one was open for 3% -> 3% of each run, Pallas kernels for 0% -> 0%
where the time goes in v1:
time: 395 us; the launch traced here: 394 us
  blocking collectives  209 us (53%)
  waiting for transfers between devices  110 us (28%)
  starting transfers between devices  19.9 us (5%)
  other arithmetic  14.7 us (4%)
  local copies, waits for them, and re-layouts  14.4 us (4%)
  between operations  14.2 us (4%)
  matrix products  11 us (3%)
    all_gather x14, blocking collectives, by_axis(): shard = jnp.sum(lax.all_gather(shard, axis), axis=0)  209 us
    reduce_scatter x2, waiting for transfers between devices, sum_in_order(): parts = lax.psum_scatter(parts, axes[k], scatter_dimension=0, tiled=True)  58.8 us
    all_to_all x2, waiting for transfers between devices, copy_for_each(): lax.all_to_all(jnp.broadcast_to(shard[None], (count, *shard.shape)), axis...  51.6 us
    all_to_all x2, starting transfers between devices, copy_for_each(): lax.all_to_all(jnp.broadcast_to(shard[None], (count, *shard.shape)), axis...  19.9 us
  transfers between devices with their start and end apart: 4, of which 3 were waited for; matrix products, arithmetic and copies ran while one was open for 3% of the time, Pallas kernels for 0%

profile of v1, /device:TPU:2, one launch (start us, length us, event | category | flops | bytes accessed | tf_op | source)
XLA Modules:
  0.0 394.1 jit_solution(11294168928086989224)
XLA Ops:
  7.2 0.0 copy-start
  7.2 2.5 broadcast_in_dim.6
  9.7 13.0 %all-to-all-start = ((bf16[32,512,64]{1,2,0:T(8,128)(2,1)}), bf16[32,512,64]{1,2,0:T(8,128)(2,1)}, u32[]{:S(2)}, u32[]{:S(2)}) async-start(bf16[32,512,64]{1,2,0:T(8,128)(2,1)} %broadcast_in_dim.6), calls=%async_computation | async-start | bytes 4194304 | tf_op jit(solution)/shard_map/all_to_all | solution.py:19
  22.8 0.0 reduce-scatter.3.cloned.1.call-start
  22.8 0.0 copy-start.3
  22.8 2.6 convert_element_type.23
  25.4 0.0 copy-done.3
  25.4 0.0 copy-start.6
  25.4 0.0 copy-start.7
  25.4 0.0 copy-start.9
  25.4 1.4 convert_element_type.24
  26.8 0.0 copy-done.6
  26.9 0.0 copy-done.7
  26.9 46.6 %all-to-all-done = bf16[32,512,64]{1,2,0:T(8,128)(2,1)} async-done(((bf16[32,512,64]{1,2,0:T(8,128)(2,1)}), bf16[32,512,64]{1,2,0:T(8,128)(2,1)}, u32[]{:S(2)}, u32[]{:S(2)}) %all-to-all-start) | async-done | bytes 2097184 | tf_op jit(solution)/shard_map/all_to_all | solution.py:19
  73.5 0.0 copy-done
  73.5 0.0 copy-done.9
  73.5 0.0 copy-start.1
  73.5 0.0 copy-start.2
  73.5 0.0 copy-start.4
  73.5 0.0 copy-start.8
  73.5 7.1 %fusion.4 = (f32[512]{0:T(512)S(1)}, f32[512]{0:T(512)S(1)}, f32[512]{0:T(512)S(1)}, f32[512]{0:T(512)S(1)}, f32[768,512]{1,0:T(8,128)S(1)}, /*index=5*/f32[768,512]{1,0:T(8,128)S(1)}, f32[768,512]{1,0:T(8,128)S(1)}) fusion(bf16[768,512]{1,0:T(8,128)(2,1)} %param.9, f32[768,512]{1,0:T(8,128)} %convert_element_type.23, f32[512]{0:T(512)S(1)} %copy-done.9, ...), kind=kOutput, calls=%fused_computation.24 | convolution fusion | flops 1618081792 | bytes 13910016 | tf_op jit(solution)/shard_map/dot_general | solution.py:97
  80.6 0.0 copy-done.1
  80.6 0.0 copy-done.2
  80.7 0.0 copy-done.4
  80.7 0.0 copy-done.8
  80.7 3.2 fusion.5
  83.9 3.9 %convolution_bitcast_fusion = f32[2048,512]{0,1:T(8,128)} fusion(bf16[768,2048]{1,0:T(8,128)(2,1)S(1)} %copy-done, f32[768,512]{1,0:T(8,128)S(1)} %get-tuple-element.23, f32[768,512]{1,0:T(8,128)S(1)} %get-tuple-element.21), kind=kOutput, calls=%fused_computation | convolution fusion | flops 1612972032 | bytes 10485760 | tf_op jit(solution)/shard_map/dot_general | solution.py:117
  87.9 5.3 %copy.21 = f32[2048,512]{1,0:T(8,128)} copy(f32[2048,512]{0,1:T(8,128)} %convolution_bitcast_fusion) | data formatting | bytes 8388608 | tf_op jit(solution)/shard_map/dot_general | solution.py:117
  93.2 4.9 %copy.22 = f32[8,4,64,512]{3,2,1,0:T(8,128)} copy(f32[8,4,64,512]{3,2,0,1:T(8,128)} %bitcast.44) | data formatting | bytes 8388608 | tf_op jit(solution)/shard_map/transpose | solution.py:37
  98.1 0.0 reduce-scatter.3.cloned.1.call-update
  98.1 0.0 reduce-scatter.5.cloned.1.call-start
  98.2 58.8 %reduce-scatter.3.cloned.1.call-done = f32[4,64,512]{2,1,0:T(8,128)} async-done(((f32[32,64,512]{2,1,0:T(8,128)}), f32[4,64,512]{2,1,0:T(8,128)}) %reduce-scatter.3.cloned.1.call-update) | async-done | bytes 524304 | tf_op jit(solution)/shard_map/reduce_scatter | solution.py:39
  157.0 0.0 reduce-scatter.5.cloned.1.call-update
  157.0 8.4 %all-gather.14 = f32[2,3,512]{2,1,0:T(4,128)S(1)} all-gather(f32[1,3,512]{2,1,0:T(4,128)S(1)} %maximum_bitcast_fusion), channel_id=2, replica_groups=mesh['rep'=2,'fs_0'=4,'fs_1'=8,'tp'=8] {'rep'}, dimensions={0}, use_global_device_ids=true | all-gather | bytes 18432 | tf_op jit(solution)/shard_map/all_gather | solution.py:30
  165.4 13.4 %all-gather.15 = f32[4,3,512]{2,1,0:T(4,128)S(1)} all-gather(f32[1,3,512]{2,1,0:T(4,128)S(1)} %bitcast.47), channel_id=3, replica_groups=mesh['rep'=2,'fs_0'=4,'fs_1'=8,'tp'=8] {'fs_0'}, dimensions={0}, use_global_device_ids=true | all-gather | bytes 30720 | tf_op jit(solution)/shard_map/all_gather | solution.py:30
  178.9 24.6 %all-gather.16 = f32[8,3,512]{2,1,0:T(4,128)S(1)} all-gather(f32[1,3,512]{2,1,0:T(4,128)S(1)} %bitcast.49), channel_id=4, replica_groups=mesh['rep'=2,'fs_0'=4,'fs_1'=8,'tp'=8] {'fs_1'}, dimensions={0}, use_global_device_ids=true | all-gather | bytes 55296 | tf_op jit(solution)/shard_map/all_gather | solution.py:30
  203.5 0.6 reduce_sum.221
  204.1 8.3 %all-gather.20 = f32[2,1,512]{2,1,0:T(1,128)S(1)} all-gather(f32[1,1,512]{2,1,0:T(1,128)S(1)} %bitcast.51), channel_id=8, replica_groups=mesh['rep'=2,'fs_0'=4,'fs_1'=8,'tp'=8] {'rep'}, dimensions={0}, use_global_device_ids=true | all-gather | bytes 6144 | tf_op jit(solution)/shard_map/all_gather | solution.py:30
  212.4 11.9 %all-gather.21 = f32[4,1,512]{2,1,0:T(1,128)S(1)} all-gather(f32[1,1,512]{2,1,0:T(1,128)S(1)} %bitcast.59), channel_id=9, replica_groups=mesh['rep'=2,'fs_0'=4,'fs_1'=8,'tp'=8] {'fs_0'}, dimensions={0}, use_global_device_ids=true | all-gather | bytes 10240 | tf_op jit(solution)/shard_map/all_gather | solution.py:30
  224.4 21.5 %all-gather.22 = f32[8,1,512]{2,1,0:T(1,128)S(1)} all-gather(f32[1,1,512]{2,1,0:T(1,128)S(1)} %bitcast.61), channel_id=10, replica_groups=mesh['rep'=2,'fs_0'=4,'fs_1'=8,'tp'=8] {'fs_1'}, dimensions={0}, use_global_device_ids=true | all-gather | bytes 18432 | tf_op jit(solution)/shard_map/all_gather | solution.py:30
  245.9 0.6 reduce_sum.231
  246.5 8.3 %all-gather.17 = f32[2,3,512]{2,1,0:T(4,128)S(1)} all-gather(f32[1,3,512]{2,1,0:T(4,128)S(1)} %maximum_bitcast_fusion.1), channel_id=5, replica_groups=mesh['rep'=2,'fs_0'=4,'fs_1'=8,'tp'=8] {'rep'}, dimensions={0}, use_global_device_ids=true | all-gather | bytes 18432 | tf_op jit(solution)/shard_map/all_gather | solution.py:30
  254.8 13.1 %all-gather.18 = f32[4,3,512]{2,1,0:T(4,128)S(1)} all-gather(f32[1,3,512]{2,1,0:T(4,128)S(1)} %bitcast.48), channel_id=6, replica_groups=mesh['rep'=2,'fs_0'=4,'fs_1'=8,'tp'=8] {'fs_0'}, dimensions={0}, use_global_device_ids=true | all-gather | bytes 30720 | tf_op jit(solution)/shard_map/all_gather | solution.py:30
  268.0 24.6 %all-gather.19 = f32[8,3,512]{2,1,0:T(4,128)S(1)} all-gather(f32[1,3,512]{2,1,0:T(4,128)S(1)} %bitcast.50), channel_id=7, replica_groups=mesh['rep'=2,'fs_0'=4,'fs_1'=8,'tp'=8] {'fs_1'}, dimensions={0}, use_global_device_ids=true | all-gather | bytes 55296 | tf_op jit(solution)/shard_map/all_gather | solution.py:30
  292.6 0.6 reduce_sum.227
  293.2 8.3 %all-gather.23 = f32[2,1,512]{2,1,0:T(1,128)S(1)} all-gather(f32[1,1,512]{2,1,0:T(1,128)S(1)} %bitcast.70), channel_id=11, replica_groups=mesh['rep'=2,'fs_0'=4,'fs_1'=8,'tp'=8] {'rep'}, dimensions={0}, use_global_device_ids=true | all-gather | bytes 6144 | tf_op jit(solution)/shard_map/all_gather | solution.py:30
  301.5 12.2 %all-gather.24 = f32[4,1,512]{2,1,0:T(1,128)S(1)} all-gather(f32[1,1,512]{2,1,0:T(1,128)S(1)} %bitcast.60), channel_id=12, replica_groups=mesh['rep'=2,'fs_0'=4,'fs_1'=8,'tp'=8] {'fs_0'}, dimensions={0}, use_global_device_ids=true | all-gather | bytes 10240 | tf_op jit(solution)/shard_map/all_gather | solution.py:30
  313.7 21.1 %all-gather.25 = f32[8,1,512]{2,1,0:T(1,128)S(1)} all-gather(f32[1,1,512]{2,1,0:T(1,128)S(1)} %bitcast.62), channel_id=13, replica_groups=mesh['rep'=2,'fs_0'=4,'fs_1'=8,'tp'=8] {'fs_1'}, dimensions={0}, use_global_device_ids=true | all-gather | bytes 18432 | tf_op jit(solution)/shard_map/all_gather | solution.py:30
  334.9 0.6 reduce_sum.235
  335.5 0.0 reduce-scatter.5.cloned.1.call-done
  335.5 1.6 broadcast_in_dim.8
  337.1 6.8 %all-to-all-start.1 = ((f32[2,64,512]{2,1,0:T(8,128)}), f32[2,64,512]{2,1,0:T(8,128)S(1)}, u32[]{:S(2)}, u32[]{:S(2)}) async-start(f32[2,64,512]{2,1,0:T(8,128)} %broadcast_in_dim.8), calls=%async_computation.3 | async-start | bytes 524288 | tf_op jit(solution)/shard_map/all_to_all | solution.py:19
  343.9 4.1 %add_convert_fusion.1 = bf16[768,512]{1,0:T(8,128)(2,1)} fusion(f32[768,512]{1,0:T(8,128)} %get-tuple-element.22, f32[512]{0:T(512)S(1)} %bitcast.67, f32[512]{0:T(512)S(1)} %bitcast.69, f32[512]{0:T(512)S(1)} %bitcast.65), kind=kLoop, calls=%fused_computation.9 | loop fusion | flops 2359296 | bytes 2365440 | tf_op jit(solution)/shard_map/convert_element_type | solution.py:102
  348.0 5.0 %all-to-all-done.1 = f32[2,64,512]{2,1,0:T(8,128)S(1)} async-done(((f32[2,64,512]{2,1,0:T(8,128)}), f32[2,64,512]{2,1,0:T(8,128)S(1)}, u32[]{:S(2)}, u32[]{:S(2)}) %all-to-all-start.1) | async-done | bytes 262176 | tf_op jit(solution)/shard_map/all_to_all | solution.py:19
  353.0 0.0 copy-start.5
  353.1 11.9 %all-gather.26 = f32[4,1,512]{2,1,0:T(1,128)S(1)} all-gather(f32[1,1,512]{2,1,0:T(1,128)S(1)} %bitcast.55), channel_id=14, replica_groups=mesh['rep'=2,'fs_0'=4,'fs_1'=8,'tp'=8] {'fs_0'}, dimensions={0}, use_global_device_ids=true | all-gather | bytes 10240 | tf_op jit(solution)/shard_map/all_gather | solution.py:30
  365.0 21.7 %all-gather.27 = f32[8,1,512]{2,1,0:T(1,128)S(1)} all-gather(f32[1,1,512]{2,1,0:T(1,128)S(1)} %bitcast.63), channel_id=15, replica_groups=mesh['rep'=2,'fs_0'=4,'fs_1'=8,'tp'=8] {'fs_1'}, dimensions={0}, use_global_device_ids=true | all-gather | bytes 18432 | tf_op jit(solution)/shard_map/all_gather | solution.py:30
  386.7 0.6 reduce_sum.239
  387.3 0.0 copy-done.5
  (15 shorter events, 0.3 us)
Async XLA Ops:
  7.2 66.3 %copy-start = (bf16[768,2048]{1,0:T(8,128)(2,1)S(1)}, bf16[768,2048]{1,0:T(8,128)(2,1)}, u32[]{:S(2)}) copy-start(bf16[768,2048]{1,0:T(8,128)(2,1)} %param.15) | copy-start | bytes 9437188
  9.7 63.8 %all-to-all-start = ((bf16[32,512,64]{1,2,0:T(8,128)(2,1)}), bf16[32,512,64]{1,2,0:T(8,128)(2,1)}, u32[]{:S(2)}, u32[]{:S(2)}) async-start(bf16[32,512,64]{1,2,0:T(8,128)(2,1)} %broadcast_in_dim.6), calls=%async_computation | async-start | bytes 4194304 | tf_op jit(solution)/shard_map/all_to_all | solution.py:19
  22.8 134.2 %reduce-scatter.3.cloned.1.call-start = ((), (), s32[]{:S(2)}) async-start(), calls=%async_computation.4 | async-start | bytes 4718592 | tf_op jit(solution)/shard_map/reduce_scatter | solution.py:39
  22.8 2.6 copy-start.3
  25.4 1.4 copy-start.6
  25.4 1.4 copy-start.7
  25.4 48.1 %copy-start.9 = (f32[512]{0:T(512)S(1)}, f32[512]{0:T(512)}, u32[]{:S(2)}) copy-start(f32[512]{0:T(512)} %param.12) | copy-start | bytes 6148
  73.5 7.1 %copy-start.1 = (f32[768,512]{1,0:T(8,128)S(1)}, f32[768,512]{1,0:T(8,128)}, u32[]{:S(2)}) copy-start(f32[768,512]{1,0:T(8,128)} %convert_element_type.23) | copy-start | bytes 4718596
  73.5 7.1 %copy-start.2 = (f32[768,512]{1,0:T(8,128)S(1)}, f32[768,512]{1,0:T(8,128)}, u32[]{:S(2)}) copy-start(f32[768,512]{1,0:T(8,128)} %convert_element_type.24) | copy-start | bytes 4718596
  73.5 7.1 %copy-start.4 = (bf16[768,512]{1,0:T(8,128)(2,1)S(1)}, bf16[768,512]{1,0:T(8,128)(2,1)}, u32[]{:S(2)}) copy-start(bf16[768,512]{1,0:T(8,128)(2,1)} %param.8) | copy-start | bytes 2359300
  73.5 7.1 %copy-start.8 = (f32[512]{0:T(512)S(1)}, f32[512]{0:T(512)}, u32[]{:S(2)}) copy-start(f32[512]{0:T(512)} %param.13) | copy-start | bytes 6148
  98.1 237.4 %reduce-scatter.5.cloned.1.call-start = ((), (), s32[]{:S(2)}) async-start(), calls=%async_computation.5 | async-start | bytes 655360 | tf_op jit(solution)/shard_map/reduce_scatter | solution.py:39
  337.1 15.9 %all-to-all-start.1 = ((f32[2,64,512]{2,1,0:T(8,128)}), f32[2,64,512]{2,1,0:T(8,128)S(1)}, u32[]{:S(2)}, u32[]{:S(2)}) async-start(f32[2,64,512]{2,1,0:T(8,128)} %broadcast_in_dim.8), calls=%async_computation.3 | async-start | bytes 524288 | tf_op jit(solution)/shard_map/all_to_all | solution.py:19
  353.0 34.3 %copy-start.5 = (f32[64,512]{1,0:T(8,128)}, f32[64,512]{1,0:T(8,128)S(1)}, u32[]{:S(2)}) copy-start(f32[64,512]{1,0:T(8,128)S(1)} %reduce_sum.236) | copy-start | bytes 393220
Sparse Core Ops, SparseCore 0:
  98.2 58.7 reduce-scatter.2
  159.8 29.2 reduce-scatter.4
